TPU v7x, 256 devices: a whole 4x4x8 slice. The times are simulated.
256 devices in a mesh: ep: 64 (over z, y, core), tp: 4 (over x).
Axes of the slice: x: 4, y: 4, z: 8, core: 2. Of those that a mesh axis runs over, the one named last changes fastest.
Arguments:
- mixer_input: bfloat16 [32768, 2048], P(('ep', 'tp')), may hold values from -6 to 6
- expert_input: bfloat16 [32768, 2048], P(('ep', 'tp')), may hold values from -6 to 6
- mixer_gain: float32 [2048], replicated, may hold values from 0.1 to 1.9
- expert_gain: float32 [2048], replicated, may hold values from 0.1 to 1.9
- query_weight: bfloat16 [2048, 1024], P(None, 'tp'), may hold values from -0.125 to 0.125
- key_weight: bfloat16 [2048, 1024], P(None, 'tp'), may hold values from -0.125 to 0.125
- value_weight: bfloat16 [2048, 1024], P(None, 'tp'), may hold values from -0.125 to 0.125
- out_weight: bfloat16 [1024, 2048], P('tp'), may hold values from -0.1875 to 0.1875
- decay_rate: float32 [8], P('tp'), may hold values from 0 to 0.12
- routing: int32 [32768, 4], P('ep'), may hold values from 0 to 63, all different within a row; in each aligned block of 128 rows (0 to 127, 128 to 255, ...) at most 12 rows name the same one
- route_weight: float32 [32768, 4], P('ep'), may hold values from 0.2 to 1
- gate_weight: bfloat16 [64, 2048, 1024], P('ep', None, 'tp'), may hold values from -0.125 to 0.125
- up_weight: bfloat16 [64, 2048, 1024], P('ep', None, 'tp'), may hold values from -0.125 to 0.125
- down_weight: bfloat16 [64, 1024, 2048], P('ep', None, 'tp'), may hold values from -0.1875 to 0.1875
- shared_gate: bfloat16 [2048, 512], P(None, 'tp'), may hold values from -0.125 to 0.125
- shared_up: bfloat16 [2048, 512], P(None, 'tp'), may hold values from -0.125 to 0.125
- shared_down: bfloat16 [512, 2048], P(None, 'tp'), may hold values from -0.25 to 0.25
Outputs:
- mixer_output: float32 [32768, 2048], P(('ep', 'tp'))
- expert_output: float32 [32768, 2048], P('ep', 'tp')
Inputs may be any that keep to these rules, and one draw needn't show every extreme that they name: `routing`: each row names 4 different experts. In each aligned block of 128 rows, no expert is named by more than 12 rows, and in some blocks one expert is named by exactly 12 rows.
All inputs are finite; a program needn't handle non-finite values.
Results may differ from a plain program's by a relative error of at most 0.0095.
Values may be sent and summed in bfloat16 or wider, within the bound.
A program may use at most 128 MiB of HBM per device.

v0:
```python
import jax
import jax.numpy as jnp
from jax import lax
from jax.sharding import Mesh
from jax.sharding import PartitionSpec as P

HD = 128
BLK = 64
EP = ("ep_0", "ep_1", "ep_2")
EP_TP = ("ep_0", "ep_1", "ep_2", "tp")
NORM_EPS = 1e-06
ROPE_BASE = 10000.0
EXACT_MATMUL = lax.Precision.HIGHEST


def nothing_yet(value, identity):
    return jax.tree.map(
        lambda a, e: jnp.broadcast_to(jnp.asarray(e, a.dtype), a.shape), value, identity
    )


def entering_2(value, axes, combine, identity):
    before = start = nothing_yet(value, identity)
    subtotal = value
    for axis in reversed(axes):
        count, mine = (lax.axis_size(axis), lax.axis_index(axis))
        pieces = jax.tree.map(lambda part: lax.all_gather(part, axis), subtotal)
        inside, subtotal = (start, start)
        for k in range(count):
            passed = k < mine
            subtotal = combine(subtotal, jax.tree.map(lambda part: part[k], pieces))
            inside = jax.tree.map(lambda new, old: jnp.where(passed, new, old), subtotal, inside)
        before = combine(inside, before)
    return before


def sent_together(arrays, axis, dim, along):
    ends, at = ([], 0)
    for a in arrays[:-1]:
        at += a.shape[along]
        ends.append(at)
    both = jnp.concatenate(arrays, axis=along)
    return tuple(jnp.split(lax.all_gather(both, axis, axis=dim, tiled=True), ends, axis=along))


def norm_rows(inputs, gain_vector):
    values = inputs.astype(jnp.float32)
    scaled = values * lax.rsqrt(jnp.mean(values * values, axis=-1, keepdims=True) + NORM_EPS)
    return (scaled * gain_vector).astype(jnp.bfloat16)


def rotate(head_rows, positions):
    head_size = head_rows.shape[-1]
    inverse = ROPE_BASE ** (-jnp.arange(0, head_size, 2, dtype=jnp.float32) / head_size)
    angles = positions[:, None] * inverse[None, :]
    cosine = jnp.cos(angles)[:, None, :]
    sine_part = jnp.sin(angles)[:, None, :]
    front_half = head_rows[..., : head_size // 2]
    behind = head_rows[..., head_size // 2 :]
    return jnp.concatenate(
        [front_half * cosine - behind * sine_part, front_half * sine_part + behind * cosine],
        axis=-1,
    )


def project(inputs, weight, head_total):
    product = jnp.dot(inputs, weight, preferred_element_type=jnp.float32).astype(jnp.bfloat16)
    product = lax.optimization_barrier(product)
    return product.astype(jnp.float32).reshape(inputs.shape[0], head_total, -1)


def chain_combine(earlier, latter):
    return (earlier[0] * latter[0], latter[0][:, None, None] * earlier[1] + latter[1])


def retain_local(query_heads, key_heads, value_heads, decay_rates):
    length, head_total, head_size = query_heads.shape
    blocks = length // BLK
    log_gamma = -decay_rates
    inner_pos = jnp.arange(BLK, dtype=jnp.float32)
    offsets = inner_pos[:, None] - inner_pos[None, :]
    inside_block_output = jnp.where(
        offsets >= 0, jnp.exp(log_gamma[:, None, None] * jnp.maximum(offsets, 0.0)), 0.0
    )
    key_scale = jnp.exp(log_gamma[None, :] * (BLK - 1.0 - inner_pos)[:, None])
    query_scale = jnp.exp(log_gamma[None, :] * (inner_pos + 1.0)[:, None])
    blocked = (blocks, BLK, head_total, head_size)
    q_blocks = query_heads.reshape(blocked)
    k_blocks = key_heads.reshape(blocked)
    v_blocks = value_heads.reshape(blocked)
    attention_scores = (
        jnp.einsum("nchd,nmhd->nhcm", q_blocks, k_blocks, precision=EXACT_MATMUL)
        * inside_block_output[None]
    )
    nearby = jnp.einsum("nhcm,nmhe->nche", attention_scores, v_blocks, precision=EXACT_MATMUL)
    block_states = jnp.einsum(
        "nchd,nche->nhde", k_blocks * key_scale[None, :, :, None], v_blocks, precision=EXACT_MATMUL
    )
    block_offset_rows = jnp.arange(blocks, dtype=jnp.float32)
    to_end = jnp.exp(log_gamma[None, :] * BLK * (blocks - 1.0 - block_offset_rows)[:, None])
    summary = jnp.einsum("nh,nhde->hde", to_end, block_states, precision=EXACT_MATMUL)
    through = jnp.exp(log_gamma * (BLK * blocks))
    incoming = entering_2(
        (through, summary), EP, chain_combine, (jnp.ones_like(through), jnp.zeros_like(summary))
    )[1]
    block_gaps = block_offset_rows[:, None] - 1.0 - block_offset_rows[None, :]
    carry_mix = jnp.where(
        block_gaps >= 0, jnp.exp(log_gamma[:, None, None] * BLK * jnp.maximum(block_gaps, 0.0)), 0.0
    )
    entering = jnp.einsum("hbj,jhde->bhde", carry_mix, block_states, precision=EXACT_MATMUL)
    entering = (
        entering
        + jnp.exp(log_gamma[None, :] * BLK * block_offset_rows[:, None])[:, :, None, None]
        * incoming[None]
    )
    distant = jnp.einsum(
        "bchd,bhde->bche",
        q_blocks * query_scale[None, :, :, None],
        entering,
        precision=EXACT_MATMUL,
    )
    retained = (nearby + distant).reshape(length, head_total, head_size)
    normed = retained * lax.rsqrt(jnp.mean(retained * retained, axis=-1, keepdims=True) + NORM_EPS)
    return normed.astype(jnp.bfloat16).reshape(length, head_total * head_size)


def assign_slots(routes, source_rows, capacity, expert_count):
    token_count, pick_count = routes.shape
    chosen = routes.reshape(token_count * pick_count)
    onehot = (chosen[:, None] == jnp.arange(expert_count, dtype=jnp.int32)[None, :]).astype(
        jnp.int32
    )
    per_source = onehot.reshape(token_count // source_rows, source_rows * pick_count, expert_count)
    earlier_hits = jnp.cumsum(per_source, axis=1) - per_source
    ranks = jnp.sum(earlier_hits * per_source, axis=2).reshape(token_count * pick_count)
    sources = jnp.arange(token_count * pick_count, dtype=jnp.int32) // (source_rows * pick_count)
    return (chosen, sources * capacity + ranks)


def gather_slots(token_rows, chosen, slot_ids, slot_count, expert_count, pick_count):
    owners = jnp.arange(chosen.shape[0], dtype=jnp.int32) // pick_count + 1
    owner_table = jnp.zeros((slot_count, expert_count), jnp.int32).at[slot_ids, chosen].set(owners)
    padded = jnp.concatenate(
        [jnp.zeros((1, token_rows.shape[1]), token_rows.dtype), token_rows], axis=0
    )
    return padded[owner_table]


def expert_hidden(routed_rows, gate_weight, up_weight):
    per_device = gate_weight.shape[0]
    grouped = routed_rows.reshape(
        routed_rows.shape[0], routed_rows.shape[1] // per_device, per_device, routed_rows.shape[2]
    )
    gate_part = jnp.einsum(
        "snxd,xdf->snxf", grouped, gate_weight, preferred_element_type=jnp.float32
    )
    up_part = jnp.einsum("snxd,xdf->snxf", grouped, up_weight, preferred_element_type=jnp.float32)
    return (jax.nn.silu(gate_part) * up_part).astype(jnp.bfloat16)


def shards(
    mixer_input,
    expert_input,
    mixer_gain,
    expert_gain,
    query_weight,
    key_weight,
    value_weight,
    out_weight,
    decay_rate,
    routing,
    route_weight,
    gate_weight,
    up_weight,
    down_weight,
    shared_gate,
    shared_up,
    shared_down,
):
    own_count = mixer_input.shape[0]
    tp_index = lax.axis_index("tp")
    own_expert_rows = norm_rows(expert_input, expert_gain)
    mixer_rows, expert_rows = sent_together(
        (norm_rows(mixer_input, mixer_gain), own_expert_rows), "tp", 0, 1
    )
    group_count = mixer_rows.shape[0]
    head_total = decay_rate.shape[0]
    positions = (
        lax.axis_index(EP) * group_count + jnp.arange(group_count, dtype=jnp.int32)
    ).astype(jnp.float32)
    query_heads = rotate(project(mixer_rows, query_weight, head_total), positions) * HD ** (-0.5)
    key_heads = rotate(project(mixer_rows, key_weight, head_total), positions)
    value_heads = project(mixer_rows, value_weight, head_total)
    mixed_heads = retain_local(query_heads, key_heads, value_heads, decay_rate)
    mixer_output = lax.psum_scatter(
        jnp.dot(mixed_heads, out_weight, preferred_element_type=jnp.float32).astype(jnp.bfloat16),
        "tp",
        scatter_dimension=0,
        tiled=True,
    ).astype(jnp.float32)
    expert_count = lax.axis_size(EP) * gate_weight.shape[0]
    pick_count = routing.shape[1]
    capacity = (3 * own_count * pick_count + 2 * expert_count - 1) // (2 * expert_count)
    chosen, slot_ids = assign_slots(routing, own_count, capacity, expert_count)
    own_span = own_count * pick_count
    own_chosen = lax.dynamic_slice_in_dim(chosen, tp_index * own_span, own_span, 0)
    own_slots = (
        lax.dynamic_slice_in_dim(slot_ids, tp_index * own_span, own_span, 0) - tp_index * capacity
    )
    outgoing = gather_slots(
        own_expert_rows, own_chosen, own_slots, capacity, expert_count, pick_count
    )
    arrived = lax.all_to_all(outgoing, EP, split_axis=1, concat_axis=1, tiled=True)
    hidden = expert_hidden(
        lax.all_gather(arrived, "tp", axis=0, tiled=True), gate_weight, up_weight
    )
    shared_hidden = (
        jax.nn.silu(jnp.dot(expert_rows, shared_gate, preferred_element_type=jnp.float32))
        * jnp.dot(expert_rows, shared_up, preferred_element_type=jnp.float32)
    ).astype(jnp.bfloat16)
    full_hidden, full_shared = (
        lax.all_gather(hidden, "tp", axis=3, tiled=True),
        lax.all_gather(shared_hidden, "tp", axis=1, tiled=True),
    )
    results = jnp.einsum(
        "snxf,xfe->snxe", full_hidden, down_weight, preferred_element_type=jnp.float32
    ).astype(jnp.bfloat16)
    results = results.reshape(results.shape[0], expert_count, results.shape[3])
    returned = lax.all_to_all(results, EP, split_axis=1, concat_axis=1, tiled=True)
    flat_results = returned.reshape(returned.shape[0] * expert_count, returned.shape[2])
    picked = flat_results[slot_ids * expert_count + chosen].astype(jnp.float32)
    weighted = jnp.sum(
        picked.reshape(group_count, pick_count, -1) * route_weight[:, :, None], axis=1
    )
    shared_result = jnp.dot(full_shared, shared_down, preferred_element_type=jnp.float32)
    expert_output = weighted + shared_result
    return (mixer_output, expert_output)


def solution(mesh):
    finer = Mesh(mesh.devices.reshape(8, 4, 2, mesh.shape["tp"]), ("ep_0", "ep_1", "ep_2", "tp"))
    placed = (
        P(EP_TP, None),
        P(EP_TP, None),
        P(),
        P(),
        P(None, "tp"),
        P(None, "tp"),
        P(None, "tp"),
        P("tp", None),
        P("tp"),
        P(EP, None),
        P(EP, None),
        P(EP, None, "tp"),
        P(EP, None, "tp"),
        P(EP, None, "tp"),
        P(None, "tp"),
        P(None, "tp"),
        P(None, "tp"),
    )
    return jax.shard_map(
        shards,
        mesh=finer,
        in_specs=placed,
        out_specs=(P(EP_TP, None), P(EP, "tp")),
        check_vma=False,
    )
```

profile of v0, /device:TPU:8, one launch (start us, length us, event | category | flops | bytes accessed | tf_op | source)
XLA Modules:
  0.0 539.4 jit_solution(6858122981832166352)
XLA Ops:
  8.7 1.2 fusion.36
  9.9 1.2 fusion.39
  11.3 4.8 reduce-window.6
  17.0 25.4 %scatter_fusion = s32[12,64]{1,0:T(8,128)S(1)} fusion(s32[12,64]{1,0:T(8,128)S(1)} %broadcast.456, s32[512]{0:T(512)S(1)} %bitcast.156, s32[512]{0:T(512)S(1)} %fusion.96), kind=kCustom, calls=%fused_computation.2 | custom fusion | bytes 10240 | tf_op jit(solution)/shard_map/scatter | solution.py:142
  42.5 1.0 fusion.38
  43.6 4.3 gather_fusion
  47.9 3.7 copy.112
  51.5 108.1 %all_to_all.10 = bf16[12,64,2048]{2,0,1:T(8,128)(2,1)S(1)} all-to-all(bf16[12,64,2048]{2,0,1:T(8,128)(2,1)S(1)} %copy.112), channel_id=1, replica_groups=mesh['ep_0'=8,'ep_1'=4,'ep_2'=2,'tp'=4] {'ep_0','ep_1','ep_2'}, dimensions={1} | all-to-all | bytes 6291456 | tf_op jit(solution)/shard_map/all_to_all | solution.py:213
  159.6 3.4 copy.113
  164.0 1.0 pad_maximum_fusion
  165.6 114.8 %all-gather.13.cloned.1.call-done = bf16[48,64,2048]{2,1,0:T(8,128)(2,1)} async-done(((bf16[12,64,2048]{2,1,0:T(8,128)(2,1)}), bf16[48,64,2048]{2,1,0:T(8,128)(2,1)}) %all-gather.13.cloned.1.call-update) | async-done | bytes 12582928 | tf_op jit(solution)/shard_map/all_gather | solution.py:215
  280.4 7.9 %fusion.43 = f32[48,64,256]{2,1,0:T(8,128)S(1)} fusion(bf16[48,64,2048]{2,1,0:T(8,128)(2,1)} %all-gather.13.cloned.1.call-done, bf16[1,2048,256]{2,1,0:T(8,128)(2,1)} %param.29), kind=kOutput, calls=%fused_computation.48 | convolution fusion | flops 3221225472 | bytes 16777216 | tf_op jit(solution)/shard_map/snxd,xdf->snxf/dot_general | solution.py:157
  288.9 5.2 fusion.2
  295.5 2.4 all-reduce.1
  299.4 8.6 %all-reduce.2 = f32[8]{0:T(128)S(1)} all-reduce(f32[8]{0:T(128)S(1)} %get-tuple-element.36), channel_id=4, replica_groups=mesh['ep_0'=8,'ep_1'=4,'ep_2'=2,'tp'=4] {'ep_1'}, use_global_device_ids=true, to_apply=%add.2 | all-reduce | flops 8 | bytes 64
  308.7 16.6 %all-gather.3 = f32[8,1,2]{2,1,0:T(1,128)S(1)} all-gather(f32[1,1,2]{2,1,0:T(1,128)S(1)} %get-tuple-element.28), channel_id=1, replica_groups=mesh['ep_0'=8,'ep_1'=4,'ep_2'=2,'tp'=4] {'ep_0'}, dimensions={0}, use_global_device_ids=true | all-gather | bytes 72 | tf_op jit(solution)/shard_map/all_gather | solution.py:27
  327.4 1.7 multiply_cosine_fusion
  329.1 5.5 %all-gather.9.cloned.1.call-done = bf16[512,4096]{1,0:T(8,128)(2,1)} async-done(((bf16[128,4096]{1,0:T(8,128)(2,1)}), bf16[512,4096]{1,0:T(8,128)(2,1)}) %all-gather.9.cloned.1.call-update) | async-done | bytes 4194320 | tf_op jit(solution)/shard_map/all_gather | solution.py:43
  334.6 2.6 fusion.24
  337.5 2.6 fusion.27
  340.3 2.6 fusion.21
  344.2 1.2 multiply_subtract_fusion.1
  345.6 1.1 fusion.54
  346.7 1.5 fusion.47
  348.2 2.2 all-gather.1
  351.2 12.8 %all_gather.47 = f32[4,2,128,128]{3,2,1,0:T(8,128)S(1)} all-gather(f32[1,2,128,128]{3,2,1,0:T(8,128)S(1)} %fusion.72), channel_id=1, replica_groups=mesh['ep_0'=8,'ep_1'=4,'ep_2'=2,'tp'=4] {'ep_1'}, dimensions={0}, use_global_device_ids=true | all-gather | bytes 655360 | tf_op jit(solution)/shard_map/all_gather | solution.py:27
  364.9 43.6 %all-gather.15.cloned.1.call-done = bf16[48,64,1,1024]{3,1,0,2:T(8,128)(2,1)} async-done(((bf16[48,64,1,256]{3,1,0,2:T(8,128)(2,1)}), bf16[48,64,1,1024]{3,1,0,2:T(8,128)(2,1)}) %all-gather.15.cloned.1.call-update) | async-done | bytes 6291472 | tf_op jit(solution)/shard_map/all_gather | solution.py:222
  408.5 6.4 %fusion.6 = bf16[48,64,512]{2,1,0:T(8,128)(2,1)S(1)} fusion(bf16[48,64,1,1024]{3,1,0,2:T(8,128)(2,1)} %all-gather.15.cloned.1.call-done, bf16[1,1024,512]{2,1,0:T(8,128)(2,1)S(1)} %copy-done), kind=kOutput, calls=%fused_computation.14 | convolution fusion | flops 3222798336 | bytes 10485760 | tf_op jit(solution)/shard_map/snxf,xfe->snxe/dot_general | solution.py:225
  414.9 3.4 copy.114
  418.3 10.9 %all-to-all-start.1 = ((bf16[48,64,512]{2,0,1:T(8,128)(2,1)}), bf16[48,64,512]{2,0,1:T(8,128)(2,1)}, u32[]{:S(2)}, u32[]{:S(2)}) async-start(bf16[48,64,512]{2,0,1:T(8,128)(2,1)} %copy.114), calls=%async_computation.2 | async-start | bytes 6291456 | tf_op jit(solution)/shard_map/all_to_all | solution.py:229
  430.0 2.3 convolution_multiply_fusion
  432.3 2.2 fusion.66
  434.5 24.3 %all-gather.11.cloned.1.call-done = f32[8,2,128,128]{3,2,1,0:T(8,128)} async-done(((f32[1,2,128,128]{3,2,1,0:T(8,128)}), f32[8,2,128,128]{3,2,1,0:T(8,128)}) %all-gather.11.cloned.1.call-update) | async-done | bytes 1048592 | tf_op jit(solution)/shard_map/all_gather | solution.py:27
  458.9 1.8 fusion.71
  460.7 1.6 fusion.19
  462.4 1.3 multiply_reduce_fusion.1
  465.0 3.4 convolution_convert_fusion
  468.8 2.3 fusion.11
  471.1 2.3 fusion.33
  473.4 18.1 %all_gather.51 = bf16[512,512]{1,0:T(8,128)(2,1)} all-gather(bf16[512,128]{1,0:T(8,128)(2,1)S(1)} %fusion.33), channel_id=1, replica_groups=mesh['ep_0'=8,'ep_1'=4,'ep_2'=2,'tp'=4] {'tp'}, dimensions={1}, use_global_device_ids=true | all-gather | bytes 655360 | tf_op jit(solution)/shard_map/all_gather | solution.py:223
  491.5 12.0 %reduce-scatter.2.cloned.1.call-done = bf16[128,2048]{1,0:T(8,128)(2,1)} async-done(((bf16[512,2048]{1,0:T(8,128)(2,1)}), bf16[128,2048]{1,0:T(8,128)(2,1)}) %reduce-scatter.2.cloned.1.call-update) | async-done | bytes 524304 | tf_op jit(solution)/shard_map/reduce_scatter | solution.py:195
  503.5 2.1 convert_element_type.78
  505.6 2.4 all-to-all-done.1
  508.1 5.3 copy.115
  513.4 9.9 %gather_fusion.1 = bf16[2048,512]{1,0:T(8,128)(2,1)S(1)} fusion(bf16[3072,512]{1,0:T(8,128)(2,1)} %bitcast.155, s32[2048]{0:T(1024)S(1)} %broadcast_clamp_fusion), kind=kCustom, calls=%fused_computation.1 | custom fusion | bytes 4202496 | tf_op jit(solution)/shard_map/gather | solution.py:231
  523.3 3.0 reshape.473
  526.3 4.9 multiply_reduce_fusion
  531.2 1.4 convolution_add_fusion
  (142 shorter events, 15.1 us)
Async XLA Ops:
  7.2 401.3 %copy-start = (bf16[1,1024,512]{2,1,0:T(8,128)(2,1)S(1)}, bf16[1,1024,512]{2,1,0:T(8,128)(2,1)}, u32[]{:S(2)}) copy-start(bf16[1,1024,512]{2,1,0:T(8,128)(2,1)} %param.30) | copy-start | bytes 3145732
  7.2 273.3 %all-gather.13.cloned.1.call-start = ((), (), s32[]{:S(2)}) async-start(), calls=%async_computation.6 | async-start | bytes 15728640 | tf_op jit(solution)/shard_map/all_gather | solution.py:215
  11.2 31.2 %copy-start.6 = (bf16[128,2048]{1,0:T(8,128)(2,1)S(1)}, bf16[128,2048]{1,0:T(8,128)(2,1)}, u32[]{:S(2)}) copy-start(bf16[128,2048]{1,0:T(8,128)(2,1)} %param.17) | copy-start | bytes 1572868
  11.2 31.2 %copy-start.12 = (f32[2048]{0:T(1024)S(1)}, f32[2048]{0:T(1024)}, u32[]{:S(2)}) copy-start(f32[2048]{0:T(1024)} %param.19) | copy-start | bytes 24580
  11.2 31.2 %copy-start.13 = (f32[2048]{0:T(1024)S(1)}, f32[2048]{0:T(1024)}, u32[]{:S(2)}) copy-start(f32[2048]{0:T(1024)} %param.20) | copy-start | bytes 24580
  16.0 26.4 %copy-start.7 = (bf16[128,2048]{1,0:T(8,128)(2,1)S(1)}, bf16[128,2048]{1,0:T(8,128)(2,1)}, u32[]{:S(2)}) copy-start(bf16[128,2048]{1,0:T(8,128)(2,1)} %param.18) | copy-start | bytes 1572868
  163.0 1.0 copy-start.9
  163.0 171.6 %all-gather.9.cloned.1.call-start = ((), (), s32[]{:S(2)}) async-start(), calls=%async_computation.3 | async-start | bytes 5242880 | tf_op jit(solution)/shard_map/all_gather | solution.py:43
  165.1 123.3 %copy-start.32 = (bf16[1,2048,256]{2,1,0:T(8,128)(2,1)S(1)}, bf16[1,2048,256]{2,1,0:T(8,128)(2,1)}, u32[]{:S(2)}) copy-start(bf16[1,2048,256]{2,1,0:T(8,128)(2,1)} %param.28) | copy-start | bytes 3145732
  165.1 243.4 %all-gather.15.cloned.1.call-start = ((), (), s32[]{:S(2)}) async-start(), calls=%async_computation.7 | async-start | bytes 7864320 | tf_op jit(solution)/shard_map/all_gather | solution.py:222
  280.4 8.5 %copy-start.31 = (bf16[48,64,2048]{2,1,0:T(8,128)(2,1)S(1)}, bf16[48,64,2048]{2,1,0:T(8,128)(2,1)}, u32[]{:S(2)}) copy-start(bf16[48,64,2048]{2,1,0:T(8,128)(2,1)} %all-gather.13.cloned.1.call-done) | copy-start | bytes 37748740
  288.9 5.2 copy-start.36
  288.9 6.5 %copy-start.28 = (f32[2]{0:T(128)S(1)}, f32[2]{0:T(128)}, u32[]{:S(2)}) copy-start(f32[2]{0:T(128)} %param.25) | copy-start | bytes 28
  288.9 9.1 %copy-start.35 = (u32[256]{0:T(256)S(1)}, u32[256]{0:T(256)}, u32[]{:S(2)}) copy-start(u32[256]{0:T(256)} %constant.162) | copy-start | bytes 3076
  294.1 164.7 %all-gather.11.cloned.1.call-start = ((), (), s32[]{:S(2)}) async-start(), calls=%async_computation.4 | async-start | bytes 1179648 | tf_op jit(solution)/shard_map/all_gather | solution.py:27
  295.5 41.7 %copy-start.15 = (f32[2]{0:T(128)}, f32[2]{0:T(128)S(1)}, u32[]{:S(2)}) copy-start(f32[2]{0:T(128)S(1)} %get-tuple-element.39) | copy-start | bytes 28
  325.3 11.9 %copy-start.29 = (f32[8]{0:T(128)}, f32[8]{0:T(128)S(1)}, u32[]{:S(2)}) copy-start(f32[8]{0:T(128)S(1)} %iota_add_fusion.2) | copy-start | bytes 100
  343.0 2.7 copy-start.3
  343.0 1.2 copy-start.10
  350.4 0.7 copy-start.4
  418.3 11.0 %copy-start.30 = (f32[8]{0:T(128)S(1)}, f32[8]{0:T(128)}, u32[]{:S(2)}) copy-start(f32[8]{0:T(128)} %copy-done.29) | copy-start | bytes 100
  418.3 89.7 %all-to-all-start.1 = ((bf16[48,64,512]{2,0,1:T(8,128)(2,1)}), bf16[48,64,512]{2,0,1:T(8,128)(2,1)}, u32[]{:S(2)}, u32[]{:S(2)}) async-start(bf16[48,64,512]{2,0,1:T(8,128)(2,1)} %copy.114), calls=%async_computation.2 | async-start | bytes 6291456 | tf_op jit(solution)/shard_map/all_to_all | solution.py:229
  429.2 29.6 %copy-start.19 = (f32[2]{0:T(128)S(1)}, f32[2]{0:T(128)}, u32[]{:S(2)}) copy-start(f32[2]{0:T(128)} %get-tuple-element.31) | copy-start | bytes 28
  429.2 29.6 %copy-start.20 = (f32[2]{0:T(128)S(1)}, f32[2]{0:T(128)}, u32[]{:S(2)}) copy-start(f32[2]{0:T(128)} %get-tuple-element.32) | copy-start | bytes 28
  429.2 29.6 %copy-start.21 = (f32[2]{0:T(128)S(1)}, f32[2]{0:T(128)}, u32[]{:S(2)}) copy-start(f32[2]{0:T(128)} %get-tuple-element.14) | copy-start | bytes 28
  429.2 29.6 %copy-start.22 = (f32[2]{0:T(128)S(1)}, f32[2]{0:T(128)}, u32[]{:S(2)}) copy-start(f32[2]{0:T(128)} %get-tuple-element.15) | copy-start | bytes 28
  429.2 29.6 %copy-start.23 = (f32[2]{0:T(128)S(1)}, f32[2]{0:T(128)}, u32[]{:S(2)}) copy-start(f32[2]{0:T(128)} %get-tuple-element.16) | copy-start | bytes 28
  429.3 29.6 %copy-start.24 = (f32[2]{0:T(128)S(1)}, f32[2]{0:T(128)}, u32[]{:S(2)}) copy-start(f32[2]{0:T(128)} %get-tuple-element.17) | copy-start | bytes 28
  429.3 29.6 %copy-start.25 = (f32[2]{0:T(128)S(1)}, f32[2]{0:T(128)}, u32[]{:S(2)}) copy-start(f32[2]{0:T(128)} %get-tuple-element.18) | copy-start | bytes 28
  429.3 29.6 %copy-start.26 = (f32[2]{0:T(128)S(1)}, f32[2]{0:T(128)}, u32[]{:S(2)}) copy-start(f32[2]{0:T(128)} %get-tuple-element.19) | copy-start | bytes 28
  429.3 31.4 %copy-start.16 = (f32[2]{0:T(128)S(1)}, f32[2]{0:T(128)}, u32[]{:S(2)}) copy-start(f32[2]{0:T(128)} %copy-done.15) | copy-start | bytes 28
  429.3 31.4 %copy-start.18 = (f32[8,2]{0,1:T(2,128)S(1)}, f32[8,2]{0,1:T(2,128)}, u32[]{:S(2)}) copy-start(f32[8,2]{0,1:T(2,128)} %get-tuple-element.26) | copy-start | bytes 196
  429.3 74.2 %reduce-scatter.2.cloned.1.call-start = ((), (), s32[]{:S(2)}) async-start(), calls=%async_computation.5 | async-start | bytes 2621440 | tf_op jit(solution)/shard_map/reduce_scatter | solution.py:195
  432.3 28.4 %copy-start.27 = (pred[8,8]{1,0:T(8,128)(4,1)S(1)}, pred[8,8]{1,0:T(8,128)(4,1)}, u32[]{:S(2)}) copy-start(pred[8,8]{1,0:T(8,128)(4,1)} %fusion.90) | copy-start | bytes 196
  432.3 30.1 %copy-start.1 = (f32[512,2,64]{2,0,1:T(8,128)S(1)}, f32[512,2,64]{2,0,1:T(8,128)}, u32[]{:S(2)}) copy-start(f32[512,2,64]{2,0,1:T(8,128)} %get-tuple-element.4) | copy-start | bytes 786436
  432.3 30.1 %copy-start.17 = (f32[64,2]{0,1:T(2,128)S(1)}, f32[64,2]{0,1:T(2,128)}, u32[]{:S(2)}) copy-start(f32[64,2]{0,1:T(2,128)} %get-tuple-element.24) | copy-start | bytes 1540
  458.8 3.6 copy-start.2
  458.9 3.6 copy-start.8
  464.9 3.6 copy-start.14
  464.9 3.9 copy-start.33
  468.4 2.7 copy-start.34
  526.3 4.9 copy-start.5
  526.3 4.9 copy-start.11
Sparse Core Ops, SparseCore 0:
  163.1 117.2 all-gather.12
  282.8 51.7 all-gather.8
  336.4 72.0 all-gather.14
  410.1 48.6 all-gather.10
  468.5 34.9 reduce-scatter.1
where the time goes:
time: 547 us; the launch traced here: 539 us
  waiting for transfers between devices  203 us (37%)
  blocking collectives  169 us (31%)
  local copies, waits for them, and re-layouts  67.4 us (12%)
  matrix products  46.5 us (9%)
  other arithmetic  26.2 us (5%)
  between operations  16.1 us (3%)
  starting transfers between devices  11.5 us (2%)
    all_gather x1, waiting for transfers between devices, shards(): lax.all_gather(arrived, 'tp', axis=0, tiled=True)  115 us
    all_to_all x1, blocking collectives, shards(): lax.all_to_all(outgoing, EP, split_axis=1, concat_axis=1, tiled=True)  108 us
    all_gather x1, waiting for transfers between devices, shards(): lax.all_gather(hidden, 'tp', axis=3, tiled=True)  43.6 us
    all_gather x3, blocking collectives, entering_2(): pieces = jax.tree.map(lambda part: lax.all_gather(part, axis), subtotal)  31.6 us
    scatter x1, local copies, waits for them, and re-layouts, gather_slots(): jnp.zeros((slot_count, expert_count), jnp.int32).at[slot_ids, chosen]  25.4 us
    all_gather x1, waiting for transfers between devices, entering_2(): pieces = jax.tree.map(lambda part: lax.all_gather(part, axis), subtotal)  24.3 us
    all_gather x1, blocking collectives, shards(): lax.all_gather(shared_hidden, 'tp', axis=1, tiled=True)  18.1 us
    reduce_scatter x1, waiting for transfers between devices, shards(): lax.psum_scatter(jnp.dot(mixed_heads, out_weight, preferred_element_type=...  12 us
  transfers between devices with their start and end apart: 6, of which 6 were waited for; matrix products, arithmetic and copies ran while one was open for 12% of the time, Pallas kernels for 0%

commit v1 on v0

--- a/solution.py
+++ b/solution.py
@@ -11,6 +11,22 @@
 NORM_EPS = 1e-06
 ROPE_BASE = 10000.0
 EXACT_MATMUL = lax.Precision.HIGHEST
+
+
+def gather_around(x, axis, dim):
+    ways, here, hop = (lax.axis_size(axis), lax.axis_index(axis), x.shape[dim])
+    shape = [n * ways if d == dim else n for d, n in enumerate(x.shape)]
+    full = lax.dynamic_update_slice_in_dim(jnp.zeros(shape, x.dtype), x, here * hop, axis=dim)
+    going_up = going_down = x
+    for far in range(1, ways // 2 + 1):
+        going_up = lax.ppermute(going_up, axis, [(d, (d + 1) % ways) for d in range(ways)])
+        full = lax.dynamic_update_slice_in_dim(full, going_up, (here - far) % ways * hop, axis=dim)
+        if 2 * far < ways:
+            going_down = lax.ppermute(going_down, axis, [(d, (d - 1) % ways) for d in range(ways)])
+            full = lax.dynamic_update_slice_in_dim(
+                full, going_down, (here + far) % ways * hop, axis=dim
+            )
+    return full
 
 
 def nothing_yet(value, identity):
@@ -219,7 +235,7 @@
         * jnp.dot(expert_rows, shared_up, preferred_element_type=jnp.float32)
     ).astype(jnp.bfloat16)
     full_hidden, full_shared = (
-        lax.all_gather(hidden, "tp", axis=3, tiled=True),
+        gather_around(hidden, "tp", 3),
         lax.all_gather(shared_hidden, "tp", axis=1, tiled=True),
     )
     results = jnp.einsum(

time: 547 us -> 508 us (0.929)
  waiting for transfers between devices: 203 us -> 157 us
  local copies, waits for them, and re-layouts: 67.4 us -> 77.3 us
    all_gather x1 -> x0, waiting for transfers between devices: 43.6 us -> none  [shards(): lax.all_gather(hidden, 'tp', axis=3, tiled=True)]
    ppermute x0 -> x3, waiting for transfers between devices: none -> 43.1 us  [the longest x2 43.1 us: gather_around(): lax.ppermute(going_up, axis, [(d, (d + 1) % ways) for d in range(ways)])]
    all_gather x1, waiting for transfers between devices: 115 us -> 80.1 us  [shards(): lax.all_gather(arrived, 'tp', axis=0, tiled=True)]
    all_gather x1, waiting for transfers between devices: 24.3 us -> 0.02 us  [entering_2(): pieces = jax.tree.map(lambda part: lax.all_gather(part, axis), subtotal)]
    all_to_all x1, waiting for transfers between devices: 2.43 us -> 21.8 us  [shards(): lax.all_to_all(results, EP, split_axis=1, concat_axis=1, tiled=True)]
    dynamic_update_slice x0 -> x3, local copies, waits for them, and re-layouts: none -> 8.55 us  [the longest x2 5.69 us: gather_around(): lax.dynamic_update_slice_in_dim(full, going_up, (here - far) % ways * hop...]
    all_gather x1, waiting for transfers between devices: 5.5 us -> 0.01 us  [sent_together(): lax.all_gather(both, axis, axis=dim, tiled=True)]
  transfers between devices with their start and end apart: 6 -> 8, of which waited for: 6 -> 5; matrix products, arithmetic and copies ran while one was open for 12% -> 19% of each run, Pallas kernels for 0% -> 0%
where the time goes in v1:
time: 508 us; the launch traced here: 500 us
  blocking collectives  168 us (33%)
  waiting for transfers between devices  157 us (31%)
  local copies, waits for them, and re-layouts  77.3 us (15%)
  matrix products  42.6 us (8%)
  other arithmetic  24.8 us (5%)
  between operations  16 us (3%)
  starting transfers between devices  14.9 us (3%)
    all_to_all x1, blocking collectives, shards(): lax.all_to_all(outgoing, EP, split_axis=1, concat_axis=1, tiled=True)  108 us
    all_gather x1, waiting for transfers between devices, shards(): lax.all_gather(arrived, 'tp', axis=0, tiled=True)  80.1 us
    ppermute x2, waiting for transfers between devices, gather_around(): lax.ppermute(going_up, axis, [(d, (d + 1) % ways) for d in range(ways)])  43.1 us
    all_gather x3, blocking collectives, entering_2(): pieces = jax.tree.map(lambda part: lax.all_gather(part, axis), subtotal)  29.2 us
    scatter x1, local copies, waits for them, and re-layouts, gather_slots(): jnp.zeros((slot_count, expert_count), jnp.int32).at[slot_ids, chosen]  25.4 us
    all_to_all x1, waiting for transfers between devices, shards(): lax.all_to_all(results, EP, split_axis=1, concat_axis=1, tiled=True)  21.8 us
    all_gather x1, blocking collectives, shards(): lax.all_gather(shared_hidden, 'tp', axis=1, tiled=True)  19.5 us
    reduce_scatter x1, waiting for transfers between devices, shards(): lax.psum_scatter(jnp.dot(mixed_heads, out_weight, preferred_element_type=...  11.8 us
  transfers between devices with their start and end apart: 8, of which 5 were waited for; matrix products, arithmetic and copies ran while one was open for 19% of the time, Pallas kernels for 0%

profile of v1, /device:TPU:8, one launch (start us, length us, event | category | flops | bytes accessed | tf_op | source)
XLA Modules:
  0.0 500.3 jit_solution(1253674713559671481)
XLA Ops:
  7.2 1.3 fusion.34
  9.8 1.5 fusion.33
  13.2 4.8 reduce-window.6
  18.9 25.4 %scatter_fusion = s32[12,64]{1,0:T(8,128)S(1)} fusion(s32[12,64]{1,0:T(8,128)S(1)} %broadcast.464, s32[512]{0:T(512)S(1)} %bitcast.161, s32[512]{0:T(512)S(1)} %fusion.91), kind=kCustom, calls=%fused_computation.2 | custom fusion | bytes 10240 | tf_op jit(solution)/shard_map/scatter | solution.py:158
  44.5 4.3 gather_fusion
  48.8 3.7 copy.112
  52.5 108.1 %all_to_all.10 = bf16[12,64,2048]{2,0,1:T(8,128)(2,1)S(1)} all-to-all(bf16[12,64,2048]{2,0,1:T(8,128)(2,1)S(1)} %copy.112), channel_id=1, replica_groups=mesh['ep_0'=8,'ep_1'=4,'ep_2'=2,'tp'=4] {'ep_0','ep_1','ep_2'}, dimensions={1} | all-to-all | bytes 6291456 | tf_op jit(solution)/shard_map/all_to_all | solution.py:229
  160.6 3.4 copy.113
  166.0 2.5 all-reduce.1
  169.9 8.6 %all-reduce.2 = f32[8]{0:T(128)S(1)} all-reduce(f32[8]{0:T(128)S(1)} %get-tuple-element.36), channel_id=4, replica_groups=mesh['ep_0'=8,'ep_1'=4,'ep_2'=2,'tp'=4] {'ep_1'}, use_global_device_ids=true, to_apply=%add.2 | all-reduce | flops 8 | bytes 64
  178.5 14.4 %all-gather.3 = f32[8,1,2]{2,1,0:T(1,128)S(1)} all-gather(f32[1,1,2]{2,1,0:T(1,128)S(1)} %get-tuple-element.28), channel_id=1, replica_groups=mesh['ep_0'=8,'ep_1'=4,'ep_2'=2,'tp'=4] {'ep_0'}, dimensions={0}, use_global_device_ids=true | all-gather | bytes 72 | tf_op jit(solution)/shard_map/all_gather | solution.py:43
  194.1 1.8 multiply_cosine_fusion
  195.9 2.3 fusion.19
  198.5 2.6 fusion.22
  201.4 80.1 %all-gather.12.cloned.1.call-done = bf16[48,64,2048]{2,1,0:T(8,128)(2,1)} async-done(((bf16[12,64,2048]{2,1,0:T(8,128)(2,1)}), bf16[48,64,2048]{2,1,0:T(8,128)(2,1)}) %all-gather.12.cloned.1.call-update) | async-done | bytes 12582928 | tf_op jit(solution)/shard_map/all_gather | solution.py:231
  281.4 7.8 %fusion.38 = f32[48,64,256]{2,1,0:T(8,128)S(1)} fusion(bf16[48,64,2048]{2,1,0:T(8,128)(2,1)} %all-gather.12.cloned.1.call-done, bf16[1,2048,256]{2,1,0:T(8,128)(2,1)} %param.29), kind=kOutput, calls=%fused_computation.50 | convolution fusion | flops 3221225472 | bytes 16777216 | tf_op jit(solution)/shard_map/snxd,xdf->snxf/dot_general | solution.py:173
  289.2 3.4 broadcast.463
  292.6 5.4 %bitcast_dynamic-update-slice_fusion.3 = (bf16[48,64,1024]{2,1,0:T(8,128)(2,1)}, bf16[48,64,1,256]{3,1,0,2:T(8,128)(2,1)}) fusion(bf16[48,64,1024]{2,1,0:T(8,128)(2,1)} %broadcast.463, s32[]{:T(128)S(6)} %select_n.297, f32[48,64,256]{2,1,0:T(8,128)S(1)} %fusion.38, bf16[48,64,2048]{2,1,0:T(8,128)(2,1)S(1)} %copy-done.17, bf16[1,2048,256]{2,1,0:T(8,128)(2,1)S(1)} %copy-done), kind=kOutput, calls=%fused_computation.26 | convolution fusion | flops 3225944064 | bytes 19922948 | tf_op jit(solution)/shard_map/snxd,xdf->snxf/dot_general | solution.py:170
  298.0 1.5 collective-permute-start
  302.0 1.8 collective-permute-start.1
  305.2 30.3 %collective-permute-done = bf16[48,64,1,256]{3,1,0,2:T(8,128)(2,1)} collective-permute-done((bf16[48,64,1,256]{3,1,0,2:T(8,128)(2,1)}, bf16[48,64,1,256]{3,1,0,2:T(8,128)(2,1)}, u32[]{:S(2)}, u32[]{:S(2)}) %collective-permute-start) | collective-permute-done | bytes 1572896 | tf_op jit(solution)/shard_map/ppermute | solution.py:22
  336.0 1.5 fusion.42
  337.5 2.0 all-gather.1
  340.2 12.8 %all_gather.44 = f32[4,2,128,128]{3,2,1,0:T(8,128)S(1)} all-gather(f32[1,2,128,128]{3,2,1,0:T(8,128)S(1)} %fusion.67), channel_id=1, replica_groups=mesh['ep_0'=8,'ep_1'=4,'ep_2'=2,'tp'=4] {'ep_1'}, dimensions={0}, use_global_device_ids=true | all-gather | bytes 655360 | tf_op jit(solution)/shard_map/all_gather | solution.py:43
  353.8 2.9 bitcast_dynamic-update-slice_fusion.2
  356.7 2.9 bitcast_dynamic-update-slice_fusion.1
  359.6 12.8 %collective-permute-done.2 = bf16[48,64,1,256]{3,1,0,2:T(8,128)(2,1)} collective-permute-done((bf16[48,64,1,256]{3,1,0,2:T(8,128)(2,1)}, bf16[48,64,1,256]{3,1,0,2:T(8,128)(2,1)}, u32[]{:S(2)}, u32[]{:S(2)}) %collective-permute-start.2) | collective-permute-done | bytes 1572896 | tf_op jit(solution)/shard_map/ppermute | solution.py:22
  372.3 2.8 bitcast_dynamic-update-slice_fusion
  375.2 6.4 %convolution_convert_fusion.1 = bf16[48,64,512]{2,1,0:T(8,128)(2,1)S(1)} fusion(bf16[48,64,1024]{2,1,0:T(8,128)(2,1)} %bitcast_dynamic-update-slice_fusion, bf16[1,1024,512]{2,1,0:T(8,128)(2,1)S(1)} %copy-done.21), kind=kOutput, calls=%fused_computation.12 | convolution fusion | flops 3222798336 | bytes 10485760 | tf_op jit(solution)/shard_map/snxf,xfe->snxe/dot_general | solution.py:241
  381.6 3.4 copy.114
  385.1 10.8 %all-to-all-start.1 = ((bf16[48,64,512]{2,0,1:T(8,128)(2,1)}), bf16[48,64,512]{2,0,1:T(8,128)(2,1)}, u32[]{:S(2)}, u32[]{:S(2)}) async-start(bf16[48,64,512]{2,0,1:T(8,128)(2,1)} %copy.114), calls=%async_computation.2 | async-start | bytes 6291456 | tf_op jit(solution)/shard_map/all_to_all | solution.py:245
  396.1 1.3 fusion.85
  398.5 1.3 fusion.61
  399.9 1.7 fusion.66
  401.6 1.6 fusion.14
  403.3 1.3 multiply_reduce_fusion.1
  405.8 3.4 convolution_convert_fusion
  409.7 2.3 fusion.6
  412.0 2.3 fusion.28
  414.3 19.5 %all_gather.47 = bf16[512,512]{1,0:T(8,128)(2,1)} all-gather(bf16[512,128]{1,0:T(8,128)(2,1)S(1)} %fusion.28), channel_id=1, replica_groups=mesh['ep_0'=8,'ep_1'=4,'ep_2'=2,'tp'=4] {'tp'}, dimensions={1}, use_global_device_ids=true | all-gather | bytes 655360 | tf_op jit(solution)/shard_map/all_gather | solution.py:239
  433.7 11.8 %reduce-scatter.2.cloned.1.call-done = bf16[128,2048]{1,0:T(8,128)(2,1)} async-done(((bf16[512,2048]{1,0:T(8,128)(2,1)}), bf16[128,2048]{1,0:T(8,128)(2,1)}) %reduce-scatter.2.cloned.1.call-update) | async-done | bytes 524304 | tf_op jit(solution)/shard_map/reduce_scatter | solution.py:211
  445.5 2.1 convert_element_type.78
  447.6 21.8 %all-to-all-done.1 = bf16[48,64,512]{2,0,1:T(8,128)(2,1)} async-done(((bf16[48,64,512]{2,0,1:T(8,128)(2,1)}), bf16[48,64,512]{2,0,1:T(8,128)(2,1)}, u32[]{:S(2)}, u32[]{:S(2)}) %all-to-all-start.1) | async-done | bytes 3145760 | tf_op jit(solution)/shard_map/all_to_all | solution.py:245
  469.5 3.6 copy.115
  473.1 9.2 %gather_fusion.1 = bf16[2048,512]{1,0:T(8,128)(2,1)} fusion(bf16[3072,512]{1,0:T(8,128)(2,1)S(1)} %bitcast.160, s32[2048]{0:T(1024)S(1)} %broadcast_clamp_fusion), kind=kCustom, calls=%fused_computation.1 | custom fusion | bytes 4202496 | tf_op jit(solution)/shard_map/gather | solution.py:247
  482.3 4.8 reshape.490
  487.2 4.9 multiply_reduce_fusion
  492.1 1.4 convolution_add_fusion
  (127 shorter events, 16.7 us)
Async XLA Ops:
  7.2 285.4 %copy-start = (bf16[1,2048,256]{2,1,0:T(8,128)(2,1)S(1)}, bf16[1,2048,256]{2,1,0:T(8,128)(2,1)}, u32[]{:S(2)}) copy-start(bf16[1,2048,256]{2,1,0:T(8,128)(2,1)} %param.28) | copy-start | bytes 3145732
  7.2 5.3 %copy-start.8 = (s32[512,4]{0,1:T(4,128)S(1)}, s32[512,4]{0,1:T(4,128)}, u32[]{:S(2)}) copy-start(s32[512,4]{0,1:T(4,128)} %param.26) | copy-start | bytes 24580
  7.2 188.7 %all-gather.8.cloned.1.call-start = ((), (), s32[]{:S(2)}) async-start(), calls=%async_computation.3 | async-start | bytes 5242880 | tf_op jit(solution)/shard_map/all_gather | solution.py:59
  12.4 269.0 %all-gather.12.cloned.1.call-start = ((), (), s32[]{:S(2)}) async-start(), calls=%async_computation.6 | async-start | bytes 15728640 | tf_op jit(solution)/shard_map/all_gather | solution.py:231
  164.0 0.7 copy-start.25
  164.0 1.9 copy-start.15
  164.0 4.5 copy-start.24
  164.0 31.9 %copy-start.19 = (bf16[2048,256]{1,0:T(8,128)(2,1)S(1)}, bf16[2048,256]{1,0:T(8,128)(2,1)}, u32[]{:S(2)}) copy-start(bf16[2048,256]{1,0:T(8,128)(2,1)} %param.21) | copy-start | bytes 3145732
  164.0 235.9 %all-gather.10.cloned.1.call-start = ((), (), s32[]{:S(2)}) async-start(), calls=%async_computation.4 | async-start | bytes 1179648 | tf_op jit(solution)/shard_map/all_gather | solution.py:43
  193.0 2.9 copy-start.16
  281.4 11.2 %copy-start.17 = (bf16[48,64,2048]{2,1,0:T(8,128)(2,1)S(1)}, bf16[48,64,2048]{2,1,0:T(8,128)(2,1)}, u32[]{:S(2)}) copy-start(bf16[48,64,2048]{2,1,0:T(8,128)(2,1)} %all-gather.12.cloned.1.call-done) | copy-start | bytes 37748740
  292.6 8.1 %copy-start.20 = (bf16[2048,256]{1,0:T(8,128)(2,1)S(1)}, bf16[2048,256]{1,0:T(8,128)(2,1)}, u32[]{:S(2)}) copy-start(bf16[2048,256]{1,0:T(8,128)(2,1)} %param.23) | copy-start | bytes 3145732
  298.0 2.7 copy-start.18
  298.0 37.5 %collective-permute-start = (bf16[48,64,1,256]{3,1,0,2:T(8,128)(2,1)}, bf16[48,64,1,256]{3,1,0,2:T(8,128)(2,1)}, u32[]{:S(2)}, u32[]{:S(2)}) collective-permute-start(bf16[48,64,1,256]{3,1,0,2:T(8,128)(2,1)} %get-tuple-element.44), channel_id=1, source_target_pairs={{0,1},{1,2},{2,3},{3,0},{4,5},{5,6},{6,7},{7,4},{8,9},{9,10},{10,1... | collective-permute-start | bytes 4718600 | tf_op jit(solution)/shard_map/ppermute | solution.py:22
  300.7 1.0 copy-start.5
  300.8 1.0 copy-start.6
  302.0 54.7 %collective-permute-start.1 = (bf16[48,64,1,256]{3,1,0,2:T(8,128)(2,1)}, bf16[48,64,1,256]{3,1,0,2:T(8,128)(2,1)}, u32[]{:S(2)}, u32[]{:S(2)}) collective-permute-start(bf16[48,64,1,256]{3,1,0,2:T(8,128)(2,1)} %get-tuple-element.44), channel_id=1, source_target_pairs={{0,3},{1,0},{2,1},{3,2},{4,7},{5,4},{6,5},{7,6},{8,11},{9,8},{10,9... | collective-permute-start | bytes 4718600 | tf_op jit(solution)/shard_map/ppermute | solution.py:25
  304.1 35.3 %copy-start.2 = (bf16[8,64,2,128]{3,2,1,0:T(2,128)(2,1)}, bf16[8,64,2,128]{3,2,1,0:T(2,128)(2,1)S(1)}, u32[]{:S(2)}) copy-start(bf16[8,64,2,128]{3,2,1,0:T(2,128)(2,1)S(1)} %reshape_reshape.3) | copy-start | bytes 786436
  335.5 36.8 %collective-permute-start.2 = (bf16[48,64,1,256]{3,1,0,2:T(8,128)(2,1)}, bf16[48,64,1,256]{3,1,0,2:T(8,128)(2,1)}, u32[]{:S(2)}, u32[]{:S(2)}) collective-permute-start(bf16[48,64,1,256]{3,1,0,2:T(8,128)(2,1)} %collective-permute-done), channel_id=1, source_target_pairs={{0,1},{1,2},{2,3},{3,0},{4,5},{5,6},{6,7},{7,4},{8,9},{9,10},{10,1... | collective-permute-start | bytes 4718600 | tf_op jit(solution)/shard_map/ppermute | solution.py:22
  339.4 0.7 copy-start.3
  356.7 18.5 %copy-start.21 = (bf16[1,1024,512]{2,1,0:T(8,128)(2,1)S(1)}, bf16[1,1024,512]{2,1,0:T(8,128)(2,1)}, u32[]{:S(2)}) copy-start(bf16[1,1024,512]{2,1,0:T(8,128)(2,1)} %param.30) | copy-start | bytes 3145732
  385.1 84.4 %all-to-all-start.1 = ((bf16[48,64,512]{2,0,1:T(8,128)(2,1)}), bf16[48,64,512]{2,0,1:T(8,128)(2,1)}, u32[]{:S(2)}, u32[]{:S(2)}) async-start(bf16[48,64,512]{2,0,1:T(8,128)(2,1)} %copy.114), calls=%async_computation.2 | async-start | bytes 6291456 | tf_op jit(solution)/shard_map/all_to_all | solution.py:245
  395.8 4.0 copy-start.10
  395.8 4.0 copy-start.11
  395.9 4.0 copy-start.12
  395.9 4.0 copy-start.13
  395.9 49.6 %reduce-scatter.2.cloned.1.call-start = ((), (), s32[]{:S(2)}) async-start(), calls=%async_computation.5 | async-start | bytes 2621440 | tf_op jit(solution)/shard_map/reduce_scatter | solution.py:211
  398.5 3.2 copy-start.14
  405.8 3.6 copy-start.9
  405.8 3.8 copy-start.22
  409.2 2.7 copy-start.23
  482.3 11.1 %copy-start.1 = (bf16[1,2048,256]{2,1,0:T(8,128)(2,1)S(1)}, bf16[1,2048,256]{2,1,0:T(8,128)(2,1)}, u32[]{:S(2)}) copy-start(bf16[1,2048,256]{2,1,0:T(8,128)(2,1)} %param.28) | copy-start | bytes 3145732
  487.2 4.9 copy-start.4
  487.2 4.9 copy-start.7
Sparse Core Ops, SparseCore 0:
  12.5 53.5 all-gather.7
  164.1 117.2 all-gather.11
  354.0 39.9 all-gather.9
  409.4 36.1 reduce-scatter.1
